TPU v7x, 32 devices: a whole 2x2x4 slice. The times are simulated.
32 devices in a mesh: sp: 16 (over z, y, x), tp: 2 (over core).
Axes of the slice: x: 2, y: 2, z: 4, core: 2. Of those that a mesh axis runs over, the one named last changes fastest.
Arguments:
- block_input: bfloat16 [8192, 2048], P('sp'), may hold values from -6 to 6
- value_weight: bfloat16 [2048, 2048], P(None, 'tp'), may hold values from -0.125 to 0.125
- queries: bfloat16 [8192, 1024], P('sp', 'tp'), may hold values from -0.5 to 0.5
- key_rows: bfloat16 [8192, 1024], P('sp', 'tp'), may hold values from -0.5 to 0.5
- log_decay: float32 [8192, 32], P('sp', 'tp'), may hold values from -0.125 to 0, as said below
- out_grad: bfloat16 [8192, 2048], P('sp', 'tp'), may hold values from -6 to 6
Outputs:
- query_grad: float32 [8192, 1024], P('sp', 'tp')
- key_grad: float32 [8192, 1024], P('sp', 'tp')
- decay_grad: float32 [8192, 32], P('sp', 'tp')
- weight_grad: float32 [2048, 2048], P('sp', 'tp')
- row_norms: float32 [2048], P('sp')
Inputs may be any that keep to these rules, and one draw needn't show every extreme that they name: `log_decay`: log decays of each position and head, never positive.
All inputs are finite; a program needn't handle non-finite values.
Results may differ from a plain program's by a relative error of at most 0.013.
Values sent between devices are 32-bit elements; how exact they have to be, the bound alone decides.
A program may use at most 128 MiB of HBM per device.

v0:
```python
import jax
import jax.numpy as jnp
from jax import lax
from jax.sharding import PartitionSpec as P

HEAD_DIM = 64
STATE = 128
SPAN = 128


exact_mode = lax.Precision.HIGHEST


def prefix(part, axis, combine, identity, reverse):
    count = lax.axis_size(axis)
    place = lax.axis_index(axis)
    ahead = count - 1 - place if reverse else place
    gathered = jax.tree.map(lambda a: lax.all_gather(a, axis), part)
    state = jax.tree.map(lambda a, e: jnp.zeros_like(a) + jnp.asarray(e, a.dtype), part, identity)

    def one(hop, state):
        source = count - 1 - hop if reverse else hop
        return combine(
            state, jax.tree.map(lambda a: lax.dynamic_index_in_dim(a, source, 0, False), gathered)
        )

    return lax.fori_loop(0, ahead, one, state)


def block_step(memory, pieces):
    queries, key_rows, decays, values = pieces
    length = decays.shape[0]
    cumulative = jnp.cumsum(decays, axis=0)
    causal = (lax.iota(jnp.int32, length)[:, None] >= lax.iota(jnp.int32, length)[None, :])[
        :, :, None, None
    ]
    log_gap = cumulative[:, None] - cumulative[None, :]
    weights = jnp.where(causal, jnp.exp(jnp.where(causal, log_gap, 0.0)), 0.0)
    scores = jnp.einsum("sgn,rgn->srg", queries, key_rows, precision=exact_mode)
    within = jnp.einsum(
        "srgj,rgjp->sgjp", scores[..., None] * weights, values, precision=exact_mode
    )
    carried = (
        jnp.einsum("sgn,gjpn->sgjp", queries, memory, precision=exact_mode)
        * jnp.exp(cumulative)[..., None]
    )
    to_end = jnp.exp(cumulative[-1] - cumulative)
    fresh_state = jnp.einsum(
        "rgn,rgjp->gjpn", key_rows, values * to_end[..., None], precision=exact_mode
    )
    new_memory = jnp.exp(cumulative[-1])[..., None, None] * memory + fresh_state
    return (new_memory, within + carried)


def combine(earlier, later):
    early_log, early_state = earlier
    late_log, late_state = later
    return (early_log + late_log, jnp.exp(late_log)[..., None, None] * early_state + late_state)


def on_device(block_input, value_weight, queries, key_rows, log_decay, out_grad):
    rows = block_input.shape[0]
    heads = log_decay.shape[1]
    groups = queries.shape[1] // STATE
    per_group = heads // groups
    blocks = rows // SPAN
    values = jnp.dot(block_input, value_weight, preferred_element_type=jnp.float32).astype(
        jnp.bfloat16
    )
    query_f = queries.astype(jnp.float32).reshape(rows, groups, STATE)
    key_f = key_rows.astype(jnp.float32).reshape(rows, groups, STATE)
    decays = log_decay.reshape(rows, groups, per_group)
    value_f = values.astype(jnp.float32).reshape(rows, groups, per_group, HEAD_DIM)
    grad_f = out_grad.astype(jnp.float32).reshape(rows, groups, per_group, HEAD_DIM)
    cumulative = jnp.cumsum(decays, axis=0)
    shard_log = cumulative[-1]
    own_state = jnp.einsum(
        "tgn,tgjp->gjpn",
        key_f,
        value_f * jnp.exp(shard_log - cumulative)[..., None],
        precision=exact_mode,
    )
    own_grad = jnp.einsum(
        "tgn,tgjp->gjpn", query_f, grad_f * jnp.exp(cumulative)[..., None], precision=exact_mode
    )
    identity = (jnp.zeros_like(shard_log), jnp.zeros_like(own_state))
    before_log, state_in = prefix((shard_log, own_state), "sp", combine, identity, False)
    unused, state_grad = prefix((shard_log, own_grad), "sp", combine, identity, True)

    def local_pass(query_in, key_in, decay_in, value_in):
        pieces = (
            query_in.reshape(blocks, SPAN, groups, STATE),
            key_in.reshape(blocks, SPAN, groups, STATE),
            decay_in.reshape(blocks, SPAN, groups, per_group),
            value_in.reshape(blocks, SPAN, groups, per_group, HEAD_DIM),
        )
        final, outputs = lax.scan(block_step, state_in, pieces)
        return (outputs, final)

    results, pullback = jax.vjp(local_pass, query_f, key_f, decays, value_f)
    query_grad, key_grad, decay_grad, value_grad = pullback(
        (grad_f.reshape(blocks, SPAN, groups, per_group, HEAD_DIM), state_grad)
    )
    rounded_grad = value_grad.reshape(rows, heads * HEAD_DIM).astype(jnp.bfloat16)
    weight_grad = lax.psum_scatter(
        lax.dot_general(
            block_input, rounded_grad, (((0,), (0,)), ((), ())), preferred_element_type=jnp.float32
        ),
        "sp",
        scatter_dimension=0,
        tiled=True,
    )
    row_norms = lax.psum(jnp.sum(weight_grad * weight_grad, axis=1), "tp")
    return (
        query_grad.reshape(rows, groups * STATE),
        key_grad.reshape(rows, groups * STATE),
        decay_grad.reshape(rows, heads),
        weight_grad,
        row_norms,
    )


def solution(mesh):
    in_specs = (
        P("sp", None),
        P(None, "tp"),
        P("sp", "tp"),
        P("sp", "tp"),
        P("sp", "tp"),
        P("sp", "tp"),
    )
    out_specs = (P("sp", "tp"), P("sp", "tp"), P("sp", "tp"), P("sp", "tp"), P("sp"))
    return jax.shard_map(
        on_device, mesh=mesh, in_specs=in_specs, out_specs=out_specs, check_vma=False
    )
```

profile of v0, /device:TPU:0, one launch (start us, length us, event | category | flops | bytes accessed | tf_op | source)
XLA Modules:
  0.0 621.7 jit_solution(10728680288372646370)
XLA Ops:
  8.2 4.8 reduce-window.6
  14.3 5.9 fusion.80
  20.2 3.0 copy.160
  23.3 3.5 fusion.76
  32.0 3.6 fusion.78
  35.7 2.9 reshape_reshape.22
  45.2 3.4 copy.164
  50.9 43.9 %all_gather.16 = f32[16,4,4]{2,1,0:T(4,128)S(1)} all-gather(f32[1,4,4]{2,1,0:T(4,128)S(1)} %copy.157), channel_id=1, replica_groups=mesh['sp'=16,'tp'=2] {'sp'}, dimensions={0}, use_global_device_ids=true | all-gather | bytes 1088 | tf_op jit(solution)/shard_map/all_gather | solution.py:18
  95.9 46.5 %all-gather.7.cloned.1.call-done = f32[64,4,64,128]{3,2,1,0:T(8,128)} async-done(((f32[4,4,64,128]{3,2,1,0:T(8,128)}), f32[64,4,64,128]{3,2,1,0:T(8,128)}) %all-gather.7.cloned.1.call-update) | async-done | bytes 8388624 | tf_op jit(solution)/shard_map/all_gather | solution.py:18
  142.6 59.3 %while.97 = (s32[]{:T(128)}, f32[4,4,64,128]{3,2,1,0:T(8,128)S(1)}, f32[4,128,128,4,4]{2,4,3,1,0:T(4,128)}, f32[4,128,128,4,4]{2,4,3,1,0:T(4,128)}, f32[4,128,12...) while((s32[]{:T(128)}, f32[4,4,64,128]{3,2,1,0:T(8,128)S(1)}, ...), condition=%wide.region_8.9_spmd.clone.clone.clone, body=%wide.region_6.8_spmd.clone.clone.sunk.clone | while | flops 505155584 | bytes 10565053 | solution.py:97
  201.9 53.9 %all-gather.5.cloned.1.call-done = f32[64,4,64,128]{3,2,1,0:T(8,128)} async-done(((f32[4,4,64,128]{3,2,1,0:T(8,128)}), f32[64,4,64,128]{3,2,1,0:T(8,128)}) %all-gather.5.cloned.1.call-update) | async-done | bytes 8388624 | tf_op jit(solution)/shard_map/all_gather | solution.py:18
  255.8 18.7 %while.95 = (s32[]{:T(128)}, f32[4,4,64,128]{3,2,1,0:T(8,128)S(1)}, s32[]{:T(128)}, f32[16,4,4]{2,1,0:T(4,128)S(1)}, f32[16,4,4,64,128]{4,3,2,1,0:T(8,128)}) while((s32[]{:T(128)}, f32[4,4,64,128]{3,2,1,0:T(8,128)S(1)}, s32[]{:T(128)}, f32[16,4,4]{2,1,0:T(4,128)S(1)}, f32[16,4,4,64,128]{4,3,2,1,0:T(8,128)}) %tuple.212), condition=%wide.region_3.4_spmd.clone, body=%wide.region_2.3_spmd.sunk.clone | while | flops 262150 | bytes 1573171 | solution.py:27
  276.9 150.5 %while.98 = (s32[]{:T(128)}, f32[4,4,64,128]{3,2,1,0:T(8,128)S(1)}, f32[4,128,4,128]{3,2,1,0:T(4,128)}, f32[4,128,4,128]{3,2,1,0:T(4,128)}, f32[4,128,4,4]{1,0,3...) while((s32[]{:T(128)}, f32[4,4,64,128]{3,2,1,0:T(8,128)S(1)}, ...), condition=%wide.region_18.19_spmd.clone.clone.clone, body=%wide.region_9.18_spmd.clone.clone.sunk.clone | while | flops 1413296128 | bytes 41144808 | solution.py:97
  285.5 4.3 fusion.190
  297.4 2.7 fusion.198
  323.0 4.3 fusion.190
  334.9 2.7 fusion.198
  360.6 4.3 fusion.190
  372.5 2.7 fusion.198
  398.2 4.3 fusion.190
  429.5 5.6 convolution_bitcast_fusion.6
  436.3 2.9 copy_bitcast_fusion.4
  439.2 169.7 %reduce-scatter.2.cloned.1.call-done = f32[128,1024]{0,1:T(8,128)} async-done(((f32[2048,1024]{0,1:T(8,128)}), f32[128,1024]{0,1:T(8,128)}) %reduce-scatter.2.cloned.1.call-update) | async-done | bytes 524304 | tf_op jit(solution)/shard_map/reduce_scatter | solution.py:105
  610.2 3.0 psum.7
  (343 shorter events, 227.9 us)
Async XLA Ops:
  7.2 7.1 %copy-start = (bf16[512,2048]{1,0:T(8,128)(2,1)S(1)}, bf16[512,2048]{1,0:T(8,128)(2,1)}, u32[]{:S(2)}) copy-start(bf16[512,2048]{1,0:T(8,128)(2,1)} %param.14) | copy-start | bytes 6291460
  7.2 135.3 %all-gather.7.cloned.1.call-start = ((), (), s32[]{:S(2)}) async-start(), calls=%async_computation.3 | async-start | bytes 8912896 | tf_op jit(solution)/shard_map/all_gather | solution.py:18
  20.2 3.0 copy-start.8
  26.9 228.9 %all-gather.5.cloned.1.call-start = ((), (), s32[]{:S(2)}) async-start(), calls=%async_computation.2 | async-start | bytes 8912896 | tf_op jit(solution)/shard_map/all_gather | solution.py:18
  35.7 573.3 %reduce-scatter.2.cloned.1.call-start = ((), (), s32[]{:S(2)}) async-start(), calls=%async_computation.1 | async-start | bytes 8912896 | tf_op jit(solution)/shard_map/reduce_scatter | solution.py:105
  38.6 4.7 copy-start.9
  45.2 3.4 copy-start.6
  45.2 4.5 copy-start.5
  301.2 6.4 %copy-start.2 = (f32[4,128,4,128]{3,1,2,0:T(8,128)S(1)}, f32[4,128,4,128]{3,1,2,0:T(8,128)}, u32[]{:S(2)}) copy-start(f32[4,128,4,128]{3,1,2,0:T(8,128)} %get-tuple-element.2150) | copy-start | bytes 3145732 | tf_op jit(solution)/shard_map/transpose(jvp())/while
  307.6 3.8 copy-start.1
  307.6 3.8 copy-start.3
  312.7 1.0 copy-start.4
  338.8 6.4 %copy-start.2 = (f32[4,128,4,128]{3,1,2,0:T(8,128)S(1)}, f32[4,128,4,128]{3,1,2,0:T(8,128)}, u32[]{:S(2)}) copy-start(f32[4,128,4,128]{3,1,2,0:T(8,128)} %get-tuple-element.2150) | copy-start | bytes 3145732 | tf_op jit(solution)/shard_map/transpose(jvp())/while
  345.2 3.8 copy-start.1
  345.2 3.8 copy-start.3
  350.3 1.0 copy-start.4
  376.4 6.4 %copy-start.2 = (f32[4,128,4,128]{3,1,2,0:T(8,128)S(1)}, f32[4,128,4,128]{3,1,2,0:T(8,128)}, u32[]{:S(2)}) copy-start(f32[4,128,4,128]{3,1,2,0:T(8,128)} %get-tuple-element.2150) | copy-start | bytes 3145732 | tf_op jit(solution)/shard_map/transpose(jvp())/while
  382.8 3.8 copy-start.1
  382.8 3.8 copy-start.3
  414.0 6.4 %copy-start.2 = (f32[4,128,4,128]{3,1,2,0:T(8,128)S(1)}, f32[4,128,4,128]{3,1,2,0:T(8,128)}, u32[]{:S(2)}) copy-start(f32[4,128,4,128]{3,1,2,0:T(8,128)} %get-tuple-element.2150) | copy-start | bytes 3145732 | tf_op jit(solution)/shard_map/transpose(jvp())/while
  420.3 3.8 copy-start.1
  420.3 3.8 copy-start.3
  425.5 1.0 copy-start.4
  435.1 1.2 copy-start.7
  (1 other events, 1.0 us)
Sparse Core Ops, SparseCore 0:
  27.0 115.4 all-gather.6
  145.3 110.4 all-gather.4
  435.2 173.7 reduce-scatter.1
where the time goes:
time: 628 us; the launch traced here: 622 us
  waiting for transfers between devices  270 us (43%)
  local copies, waits for them, and re-layouts  114 us (18%)
  matrix products  105 us (17%)
  other arithmetic  69.2 us (11%)
  blocking collectives  46.8 us (7%)
  between operations  13.9 us (2%)
    reduce_scatter x1, waiting for transfers between devices, on_device(): lax.psum_scatter(lax.dot_general(block_input, rounded_grad, (((0,), (0,))...  170 us
    all_gather x2, waiting for transfers between devices, prefix(): gathered = jax.tree.map(lambda a: lax.all_gather(a, axis), part)  100 us
    all_gather x1, blocking collectives, prefix(): gathered = jax.tree.map(lambda a: lax.all_gather(a, axis), part)  43.9 us
    dynamic_slice x40, local copies, waits for them, and re-layouts, local_pass(): final, outputs = lax.scan(block_step, state_in, pieces)  43.3 us
    dot_general x12, matrix products, block_step(): jnp.einsum('rgn,rgjp->gjpn', key_rows, values * to_end[..., None], precis...  25.7 us
    dot_general x8, matrix products, block_step(): jnp.einsum('srgj,rgjp->sgjp', scores[..., None] * weights, values, precis...  22.7 us
    dynamic_update_slice x48, local copies, waits for them, and re-layouts, local_pass(): final, outputs = lax.scan(block_step, state_in, pieces)  21.6 us
    dot_general x12, matrix products, block_step(): jnp.einsum('sgn,gjpn->sgjp', queries, memory, precision=exact_mode)  20.7 us
  transfers between devices with their start and end apart: 3, of which 3 were waited for; matrix products, arithmetic and copies ran while one was open for 14% of the time, Pallas kernels for 0%

commit v1 on v0

v1 whole, which is shorter than its diff:
```python
import functools

import jax
import jax.numpy as jnp
from jax import lax
from jax.experimental import pallas as pl
from jax.experimental.pallas import tpu as pltpu
from jax.sharding import PartitionSpec as P

HEAD_DIM = 64
STATE = 128
SPAN = 128
LANES = 128

F32 = jnp.float32
BF16 = jnp.bfloat16
HI = lax.Precision.HIGHEST
VMEM = pltpu.VMEM
MESH = pl.DeviceIdType.MESH
GRANT = 60 * 1024 * 1024


def dot(a, b, ca, cb, precision=None):
    return lax.dot_general(
        a, b, (((ca,), (cb,)), ((), ())), precision=precision, preferred_element_type=F32
    )


def square(size, test):
    rows = lax.broadcasted_iota(jnp.int32, (size, size), 0)
    cols = lax.broadcasted_iota(jnp.int32, (size, size), 1)
    return test(rows, cols)


def spread(columns, width):
    length, heads = columns.shape
    lane = lax.broadcasted_iota(jnp.int32, (length, width), 1)
    out = jnp.broadcast_to(columns[:, 0:1], (length, width))
    for j in range(1, heads):
        out = jnp.where(lane >= j * HEAD_DIM, columns[:, j : j + 1], out)
    return out


def own_kernel(x, w, q, k, ld, g, values, fresh, back, logs):
    rows = x.shape[0]
    heads = ld.shape[1]
    width = heads * HEAD_DIM
    tri = square(SPAN, lambda r, c: r >= c).astype(F32)
    v = dot(x[...], w[...], 1, 0).astype(BF16)
    values[...] = v
    pieces = []
    total = jnp.zeros((1, heads), F32)
    for c in range(rows // SPAN):
        cum = dot(tri, ld[0, :, c * SPAN : (c + 1) * SPAN], 1, 1, HI) + total
        total = cum[SPAN - 1 : SPAN, :]
        pieces.append(cum)
    state = jnp.zeros((width, STATE), F32)
    grad = jnp.zeros((width, STATE), F32)
    for c in range(rows // SPAN):
        at = slice(c * SPAN, (c + 1) * SPAN)
        to_end = spread(jnp.exp(total - pieces[c]), width)
        ve = (v[at, :].astype(F32) * to_end).astype(BF16)
        ge = (g[at, :].astype(F32) * spread(jnp.exp(pieces[c]), width)).astype(BF16)
        state = state + dot(ve, k[at, :], 0, 0)
        grad = grad + dot(ge, q[at, :], 0, 0)
    fresh[...] = state
    back[...] = grad
    for j in range(heads):
        logs[j] = jnp.broadcast_to(total[:, j : j + 1], logs.shape[1:])


def scan_kernel(n, chunk, fresh, back, logs, before, after,
                got_f, got_b, got_l, send_f, send_b, sems_out, sems_in, sems_out2, sems_in2):
    me = lax.axis_index("sp")
    per_head = HEAD_DIM // chunk

    barrier = pltpu.get_barrier_semaphore()

    def greet(d, _):
        pl.semaphore_signal(barrier, inc=1, device_id={"sp": lax.rem(me + d, n)}, device_id_type=MESH)
        return 0

    lax.fori_loop(1, n, greet, 0)
    pl.semaphore_wait(barrier, n - 1)

    def first(d):
        to = lax.rem(me + d, n)
        return [
            pltpu.make_async_remote_copy(
                src, dst, sems_out.at[kind, d], sems_in.at[kind, d],
                device_id={"sp": to}, device_id_type=MESH,
            )
            for kind, (src, dst) in enumerate((
                (fresh.at[to], got_f.at[me]),
                (back.at[to], got_b.at[me]),
                (logs.at[to // per_head], got_l.at[me]),
            ))
        ]

    def go(make):
        def body(d, _):
            for copy in make(d):
                copy.start()
            return 0
        lax.fori_loop(1, n, body, 0)

    def done(make):
        def body(d, _):
            for copy in make(d):
                copy.wait()
            return 0
        lax.fori_loop(1, n, body, 0)

    go(first)
    got_f[me] = fresh[me]
    got_b[me] = back[me]
    got_l[me] = logs[me // per_head]
    done(first)

    def forward(j, run):
        send_f[j] = run
        return jnp.exp(got_l[j][0:1, :]) * run + got_f[j]

    def backward(i, run):
        j = n - 1 - i
        send_b[j] = run
        return jnp.exp(got_l[j][0:1, :]) * run + got_b[j]

    zero = jnp.zeros((chunk, STATE), F32)
    lax.fori_loop(0, n, forward, zero)
    lax.fori_loop(0, n, backward, zero)

    def second(d):
        to = lax.rem(me + d, n)
        return [
            pltpu.make_async_remote_copy(
                src, dst, sems_out2.at[kind, d], sems_in2.at[kind, d],
                device_id={"sp": to}, device_id_type=MESH,
            )
            for kind, (src, dst) in enumerate((
                (send_b.at[to], after.at[me]),
                (send_f.at[to], before.at[me]),
            ))
        ]

    go(second)
    before[me] = send_f[me]
    after[me] = send_b[me]
    done(second)


def grad_kernel(q, k, v, g, ld, first_state, last_grad, dq, dk, dv, dd, states):
    rows = q.shape[0]
    heads = ld.shape[1]
    width = heads * HEAD_DIM
    blocks = rows // SPAN
    causal = square(SPAN, lambda r, c: r >= c)
    tri = causal.astype(F32)
    strict = square(SPAN, lambda r, c: r < c).astype(F32)
    lane = lax.broadcasted_iota(jnp.int32, (heads, width), 1)
    pick = ((lane >= HEAD_DIM * lax.broadcasted_iota(jnp.int32, (heads, width), 0))
            & (lane < HEAD_DIM * (1 + lax.broadcasted_iota(jnp.int32, (heads, width), 0)))).astype(F32)

    def sums(c):
        part = ld[0, :, c * SPAN : (c + 1) * SPAN]
        return dot(tri, part, 1, 1, HI), dot(part, tri, 1, 1, HI)

    def shrink(row, state):
        return jnp.concatenate(
            [jnp.exp(row[j : j + 1, SPAN - 1 : SPAN]) * state[j * HEAD_DIM : (j + 1) * HEAD_DIM]
             for j in range(heads)], axis=0)

    cums = [sums(c) for c in range(blocks)]
    states[0] = first_state[...]
    for c in range(blocks - 1):
        at = slice(c * SPAN, (c + 1) * SPAN)
        col, row = cums[c]
        to_end = spread(jnp.exp(col[SPAN - 1 : SPAN, :] - col), width)
        ve = (v[at, :].astype(F32) * to_end).astype(BF16)
        states[c + 1] = shrink(row, states[c]) + dot(ve, k[at, :], 0, 0)
    d_state = last_grad[...]
    for c in reversed(range(blocks)):
        at = slice(c * SPAN, (c + 1) * SPAN)
        col, row = cums[c]
        qc, kc = q[at, :], k[at, :]
        vc, gc = v[at, :], g[at, :]
        state = states[c]
        sb, db = state.astype(BF16), d_state.astype(BF16)
        to_end = spread(jnp.exp(col[SPAN - 1 : SPAN, :] - col), width)
        ge32 = gc.astype(F32) * spread(jnp.exp(col), width)
        v32 = vc.astype(F32)
        ge = ge32.astype(BF16)
        ve = (v32 * to_end).astype(BF16)
        y = dot(qc, sb, 1, 1)
        z = dot(kc, db, 1, 1) * to_end
        r_cross = dot(pick, ge32 * y, 1, 1, HI)
        c_cross = dot(pick, v32 * z, 1, 1, HI)
        scores = dot(qc, kc, 1, 1)
        d_scores = jnp.zeros((SPAN, SPAN), F32)
        r_in, c_in, d_values, through = [], [], [], []
        kept = shrink(row, state)
        for j in range(heads):
            head = slice(j * HEAD_DIM, (j + 1) * HEAD_DIM)
            gap = jnp.minimum(col[:, j : j + 1] - row[j : j + 1, :], 0.0)
            weight = jnp.where(causal, jnp.exp(gap), 0.0)
            t1 = dot(gc[:, head], vc[:, head], 1, 1) * weight
            d_scores = d_scores + t1
            pairs = t1 * scores
            r_in.append(jnp.sum(pairs, axis=1, keepdims=True))
            c_in.append(jnp.sum(pairs, axis=0, keepdims=True))
            d_values.append(dot((scores * weight).astype(BF16), gc[:, head], 0, 0))
            through.append(jnp.sum(kept[head, :] * d_state[head, :], keepdims=True))
        dv[at, :] = (jnp.concatenate(d_values, axis=1) + z).astype(BF16)
        dsb = d_scores.astype(BF16)
        dq[at, :] = dot(dsb, kc, 1, 0) + dot(ge, sb, 1, 0)
        dk[at, :] = dot(dsb, qc, 0, 0) + dot(ve, db, 1, 0)
        r_rows = dot(jnp.concatenate(r_in, axis=1), tri, 0, 0, HI)
        rest = dot(r_cross - jnp.concatenate(c_in, axis=0), tri, 1, 0, HI)
        dd[0, :, at] = (r_rows + rest + dot(c_cross, strict, 1, 0, HI)
                        + jnp.concatenate(through, axis=0))
        d_state = shrink(row, d_state) + dot(ge, qc, 0, 0)


def bits_of(n):
    return n.bit_length() - 1


def order_of(stream, bits):
    lead = min(3, bits)
    turn = stream % lead if lead else 0
    return [(turn + i) % lead for i in range(lead)] + list(range(lead, bits))


def weight_kernel(n, xt, dv, out, part, *rest):
    bits = bits_of(n)
    levels, (send, recv) = rest[:bits], rest[bits:]
    streams = part.shape[0]
    me = lax.axis_index("sp")
    mine = [lax.rem(me // (1 << b), 2) for b in range(bits)]
    partner = [me + (1 << b) * (1 - 2 * mine[b]) for b in range(bits)]

    barrier = pltpu.get_barrier_semaphore()
    for b in range(bits):
        pl.semaphore_signal(barrier, inc=1, device_id={"sp": partner[b]}, device_id_type=MESH)
    pl.semaphore_wait(barrier, bits)

    def fill(s, spots):
        order = order_of(s, bits)
        cols = dv[:, s * LANES : (s + 1) * LANES]
        for spot in spots:
            block = 0
            for place, b in enumerate(order):
                flip = (spot >> (bits - 1 - place)) & 1
                block = block + (1 << b) * ((1 - mine[b]) if flip else mine[b])
            part[s, spot] = dot(xt[block], cols, 1, 0)

    def hop(s, step):
        src = part if step == 0 else levels[step - 1]
        half = n >> (step + 1)
        return pltpu.make_async_remote_copy(
            src.at[s, pl.ds(half, half)], levels[step].at[s],
            send.at[s, step], recv.at[s, step],
            device_id={"sp": partner[order_of(s, bits)[step]]}, device_id_type=MESH,
        )

    for s in range(streams):
        fill(s, range(n // 2, n))
        hop(s, 0).start()
    for s in range(streams):
        fill(s, range(n // 2))
    for step in range(bits):
        half = n >> (step + 1)
        src = part if step == 0 else levels[step - 1]
        for s in range(streams):
            hop(s, step).wait_recv()
            if step == bits - 1:
                out[:, s * LANES : (s + 1) * LANES] = src[s, 0] + levels[step][s, 0]
            else:
                levels[step][s] = levels[step][s] + src[s, 0:half]
                hop(s, step + 1).start()
    for step in range(bits):
        for s in range(streams):
            hop(s, step).wait_send()


def on_device(n, block_input, value_weight, queries, key_rows, log_decay, out_grad):
    rows, model = block_input.shape
    heads = log_decay.shape[1]
    groups = queries.shape[1] // STATE
    per_group = heads // groups
    width = per_group * HEAD_DIM
    chunk = heads * HEAD_DIM // n
    blocks = rows // SPAN
    decays = log_decay.T.reshape(groups, per_group, rows)
    xt = block_input.T.reshape(n, model // n, rows)

    def by_group(cols):
        return pl.BlockSpec((rows, cols), lambda i: (0, i))

    ld_spec = pl.BlockSpec((1, per_group, rows), lambda i: (i, 0, 0))
    state_spec = pl.BlockSpec((width, STATE), lambda i: (i, 0))
    state_shape = jax.ShapeDtypeStruct((heads * HEAD_DIM, STATE), F32)
    values, fresh, back, logs = pl.pallas_call(
        own_kernel,
        grid=(groups,),
        in_specs=[
            pl.BlockSpec((rows, model), lambda i: (0, 0)),
            pl.BlockSpec((model, width), lambda i: (0, i)),
            by_group(STATE), by_group(STATE), ld_spec, by_group(width),
        ],
        out_specs=[
            by_group(width), state_spec, state_spec,
            pl.BlockSpec((per_group, 8, LANES), lambda i: (i, 0, 0)),
        ],
        out_shape=[
            jax.ShapeDtypeStruct((rows, heads * HEAD_DIM), BF16), state_shape, state_shape,
            jax.ShapeDtypeStruct((heads, 8, LANES), F32),
        ],
        compiler_params=pltpu.CompilerParams(vmem_limit_bytes=GRANT),
        name="own_states",
    )(block_input, value_weight, queries, key_rows, decays, out_grad)

    vm = pl.BlockSpec(memory_space=VMEM)
    piece = (n, chunk, STATE)
    before, after = pl.pallas_call(
        functools.partial(scan_kernel, n, chunk),
        in_specs=[vm] * 3,
        out_specs=[vm] * 2,
        out_shape=[jax.ShapeDtypeStruct(piece, F32)] * 2,
        scratch_shapes=[VMEM(piece, F32)] * 2 + [VMEM((n, 8, LANES), F32)] + [VMEM(piece, F32)] * 2
        + [pltpu.SemaphoreType.DMA((3, n))] * 2 + [pltpu.SemaphoreType.DMA((2, n))] * 2,
        compiler_params=pltpu.CompilerParams(collective_id=0, has_side_effects=True, vmem_limit_bytes=GRANT),
        name="scan_states",
    )(fresh.reshape(piece), back.reshape(piece), logs)

    query_grad, key_grad, rounded_grad, decay_rows = pl.pallas_call(
        grad_kernel,
        grid=(groups,),
        in_specs=[by_group(STATE), by_group(STATE), by_group(width), by_group(width), ld_spec,
                  state_spec, state_spec],
        out_specs=[by_group(STATE), by_group(STATE), by_group(width), ld_spec],
        out_shape=[
            jax.ShapeDtypeStruct(queries.shape, F32), jax.ShapeDtypeStruct(queries.shape, F32),
            jax.ShapeDtypeStruct((rows, heads * HEAD_DIM), BF16),
            jax.ShapeDtypeStruct((groups, per_group, rows), F32),
        ],
        scratch_shapes=[VMEM((blocks, width, STATE), F32)],
        compiler_params=pltpu.CompilerParams(vmem_limit_bytes=GRANT),
        name="mixer_grads",
    )(queries, key_rows, values, out_grad, decays,
      before.reshape(heads * HEAD_DIM, STATE), after.reshape(heads * HEAD_DIM, STATE))

    own_rows, columns = model // n, heads * HEAD_DIM
    streams = columns // LANES
    bits = bits_of(n)
    weight_grad = pl.pallas_call(
        functools.partial(weight_kernel, n),
        in_specs=[vm] * 2,
        out_specs=vm,
        out_shape=jax.ShapeDtypeStruct((own_rows, columns), F32),
        scratch_shapes=[VMEM((streams, n, own_rows, LANES), F32)]
        + [VMEM((streams, n >> (b + 1), own_rows, LANES), F32) for b in range(bits)]
        + [pltpu.SemaphoreType.DMA((streams, bits))] * 2,
        compiler_params=pltpu.CompilerParams(collective_id=1, has_side_effects=True, vmem_limit_bytes=GRANT),
        name="weight_grad",
    )(xt, rounded_grad)
    row_norms = lax.psum(jnp.sum(weight_grad * weight_grad, axis=1), "tp")
    return query_grad, key_grad, decay_rows.reshape(heads, rows).T, weight_grad, row_norms


def solution(mesh):
    in_specs = (
        P("sp", None),
        P(None, "tp"),
        P("sp", "tp"),
        P("sp", "tp"),
        P("sp", "tp"),
        P("sp", "tp"),
    )
    out_specs = (P("sp", "tp"), P("sp", "tp"), P("sp", "tp"), P("sp", "tp"), P("sp"))
    return jax.shard_map(
        functools.partial(on_device, mesh.shape["sp"]),
        mesh=mesh, in_specs=in_specs, out_specs=out_specs, check_vma=False,
    )
```

time: 628 us -> 195 us (0.31)
  waiting for transfers between devices: 270 us -> 0 us
  Pallas kernels: 0 us -> 183 us
  local copies, waits for them, and re-layouts: 114 us -> 7.17 us
  matrix products: 105 us -> 0 us
  other arithmetic: 69.2 us -> 1.16 us
  blocking collectives: 46.8 us -> 2.97 us
  between operations: 13.9 us -> 0.66 us
    pallas_call x0 -> x4, Pallas kernels: none -> 183 us  [the longest x1 95.8 us: on_device(): pl.pallas_call(functools.partial(weight_kernel, n), in_specs=[vm] * 2, ou...]
    reduce_scatter x1 -> x0, waiting for transfers between devices: 170 us -> none  [on_device(): lax.psum_scatter(lax.dot_general(block_input, rounded_grad, (((0,), (0,))...]
    dot_general x48 -> x0, matrix products: 105 us -> none  [the longest x12 25.7 us: block_step(): jnp.einsum('rgn,rgjp->gjpn', key_rows, values * to_end[..., None], precis...]
    all_gather x2 -> x0, waiting for transfers between devices: 100 us -> none  [prefix(): gathered = jax.tree.map(lambda a: lax.all_gather(a, axis), part)]
    all_gather x1 -> x0, blocking collectives: 43.9 us -> none  [prefix(): gathered = jax.tree.map(lambda a: lax.all_gather(a, axis), part)]
    dynamic_slice x40 -> x0, local copies, waits for them, and re-layouts: 43.3 us -> none  [local_pass(): final, outputs = lax.scan(block_step, state_in, pieces)]
    dynamic_update_slice x48 -> x0, local copies, waits for them, and re-layouts: 21.6 us -> none  [local_pass(): final, outputs = lax.scan(block_step, state_in, pieces)]
    another operation x24 -> x0, other arithmetic: 20.3 us -> none  [the longest x12 14.7 us: block_step(): cumulative = jnp.cumsum(decays, axis=0)]
  transfers between devices with their start and end apart: 3 -> 0, of which waited for: 3 -> 0; matrix products, arithmetic and copies ran while one was open for 14% -> 0% of each run, Pallas kernels for 0% -> 0%
where the time goes in v1:
time: 195 us
  Pallas kernels  183 us (94%)
  local copies, waits for them, and re-layouts  7.17 us (4%)
  blocking collectives  2.97 us (2%)
    pallas_call x1, Pallas kernels, on_device(): pl.pallas_call(functools.partial(weight_kernel, n), in_specs=[vm] * 2, ou...  95.8 us
    pallas_call x1, Pallas kernels, on_device(): pl.pallas_call(functools.partial(scan_kernel, n, chunk), in_specs=[vm] *...  53.5 us
    pallas_call x1, Pallas kernels, on_device(): pl.pallas_call(grad_kernel, grid=(groups,), in_specs=[by_group(STATE), by...  23.7 us
    pallas_call x1, Pallas kernels, on_device(): pl.pallas_call(own_kernel, grid=(groups,), in_specs=[pl.BlockSpec((rows,...  9.85 us

profile of v1, /device:TPU:0, one launch (start us, length us, event | category | flops | bytes accessed | tf_op | source)
XLA Modules:
  0.0 194.8 jit_solution(1333633378044441828)
XLA Ops:
  0.6 1.4 reshape.31.ld
  2.0 9.9 %own_states.1 = (bf16[512,1024]{1,0:T(8,128)(2,1)}, f32[1024,128]{1,0:T(8,128)}, f32[1024,128]{1,0:T(8,128)}, f32[16,8,128]{2,1,0:T(8,128)}) custom-call(bf16[512,2048]{1,0:T(8,128)(2,1)} %x.1, bf16[2048,1024]{1,0:T(8,128)(2,1)} %w.1, bf16[512,512]{1,0:T(8,128)(2,1)} %q.3, bf16[512,512]{1,0:T(8,128)(2,1)} %k.3, f32[4,4,512]{2,1,0:T(4,128)} %reshape.31.ld, ...), custom_call_target="tpu_custom_call" | custom-call | tf_op jit(solution)/shard_map/own_states/pallas_call | solution.py:303
  11.9 53.5 %scan_states.1 = (f32[16,64,128]{2,1,0:T(8,128)}, f32[16,64,128]{2,1,0:T(8,128)}) custom-call(f32[16,64,128]{2,1,0:T(8,128)} %bitcast.10, f32[16,64,128]{2,1,0:T(8,128)} %bitcast.11, f32[16,8,128]{2,1,0:T(8,128)} %get-tuple-element.18.logs), custom_call_target="tpu_custom_call" | custom-call | tf_op jit(solution)/shard_map/scan_states/pallas_call | solution.py:325
  65.3 0.0 copy-start
  65.4 23.7 %mixer_grads.1 = (f32[512,512]{1,0:T(8,128)}, f32[512,512]{1,0:T(8,128)}, bf16[512,1024]{1,0:T(8,128)(2,1)}, f32[4,4,512]{2,1,0:T(4,128)}) custom-call(bf16[512,512]{1,0:T(8,128)(2,1)} %q.3, bf16[512,512]{1,0:T(8,128)(2,1)} %k.3, bf16[512,1024]{1,0:T(8,128)(2,1)} %get-tuple-element.15.v, bf16[512,1024]{1,0:T(8,128)(2,1)} %g.3, f32[4,4,512]{2,1,0:T(4,128)} %reshape.31.ld, ...), custom_call_target="tpu_custom_call" | custom-call | tf_op jit(solution)/shard_map/mixer_grads/pallas_call | solution.py:336
  89.0 1.4 reshape.36
  90.4 0.0 copy-done
  90.4 2.5 %copy.11 = bf16[2048,512]{1,0:T(8,128)(2,1)} copy(bf16[2048,512]{0,1:T(8,128)(2,1)S(1)} %bitcast.9) | data formatting | bytes 4194304 | tf_op jit(solution)/shard_map/transpose | solution.py:295
  92.9 95.8 %weight_grad.1 = f32[128,1024]{1,0:T(8,128)} custom-call(bf16[16,128,512]{2,1,0:T(8,128)(2,1)} %bitcast.8, bf16[512,1024]{1,0:T(8,128)(2,1)} %get-tuple-element.24.dv), custom_call_target="tpu_custom_call" | custom-call | tf_op jit(solution)/shard_map/weight_grad/pallas_call | solution.py:356
  188.7 1.2 multiply_reduce_fusion
  189.9 3.0 %psum.7 = f32[128]{0:T(128)} all-reduce(f32[128]{0:T(128)S(1)} %multiply_reduce_fusion), channel_id=1, replica_groups=mesh['sp'=16,'tp'=2] {'tp'}, use_global_device_ids=true, to_apply=%region_1.0 | all-reduce | flops 128 | bytes 1024 | tf_op jit(solution)/shard_map/psum | solution.py:367
  192.9 1.9 copy.13
Async XLA Ops:
  65.3 25.1 %copy-start = (bf16[512,2048]{1,0:T(8,128)(2,1)S(1)}, bf16[512,2048]{1,0:T(8,128)(2,1)}, u32[]{:S(2)}) copy-start(bf16[512,2048]{1,0:T(8,128)(2,1)} %x.1) | copy-start | bytes 6291460

commit v2 on v1

--- a/solution.py
+++ b/solution.py
@@ -149,76 +149,100 @@
     done(second)
 
 
-def grad_kernel(q, k, v, g, ld, first_state, last_grad, dq, dk, dv, dd, states):
-    rows = q.shape[0]
+def loop_blocks(q, k, v, g, ld, i):
     heads = ld.shape[1]
     width = heads * HEAD_DIM
-    blocks = rows // SPAN
     causal = square(SPAN, lambda r, c: r >= c)
     tri = causal.astype(F32)
+
+    def read(c):
+        at = pl.ds(pl.multiple_of(c * SPAN, SPAN), SPAN)
+        part = ld[i, :, at]
+        col, row = dot(tri, part, 1, 1, HI), dot(part, tri, 1, 1, HI)
+        lanes = slice(i * STATE, (i + 1) * STATE)
+        wide = slice(i * width, (i + 1) * width)
+        to_end = spread(jnp.exp(col[SPAN - 1 : SPAN, :] - col), width)
+        grown = spread(jnp.exp(col), width)
+        return at, col, row, q[at, lanes], k[at, lanes], v[at, wide], g[at, wide], to_end, grown
+
+    def weight(col, row, j):
+        gap = jnp.minimum(col[:, j : j + 1] - row[j : j + 1, :], 0.0)
+        return jnp.where(causal, jnp.exp(gap), 0.0)
+
+    return heads, width, tri, read, weight
+
+
+def shrink(row, state):
+    return jnp.concatenate(
+        [jnp.exp(row[j : j + 1, SPAN - 1 : SPAN]) * state[j * HEAD_DIM : (j + 1) * HEAD_DIM]
+         for j in range(row.shape[0])], axis=0)
+
+
+def value_pass(refs, i, last_grad, dv, grads):
+    q, k, v, g, ld = refs
+    heads, width, tri, read, weight = loop_blocks(q, k, v, g, ld, i)
+    blocks = q.shape[0] // SPAN
+
+    def one(step, d_state):
+        c = blocks - 1 - step
+        at, col, row, qc, kc, vc, gc, to_end, grown = read(c)
+        grads[i, c] = d_state
+        z = dot(kc, d_state.astype(BF16), 1, 1) * to_end
+        scores = dot(qc, kc, 1, 1)
+        parts = [
+            dot((scores * weight(col, row, j)).astype(BF16),
+                gc[:, j * HEAD_DIM : (j + 1) * HEAD_DIM], 0, 0)
+            for j in range(heads)
+        ]
+        dv[at, i * width : (i + 1) * width] = (jnp.concatenate(parts, axis=1) + z).astype(BF16)
+        ge = (gc.astype(F32) * grown).astype(BF16)
+        return shrink(row, d_state) + dot(ge, qc, 0, 0)
+
+    lax.fori_loop(0, blocks, one, last_grad[i * width : (i + 1) * width, :])
+
+
+def rest_pass(refs, i, first_state, grads, dq, dk, dd):
+    q, k, v, g, ld = refs
+    heads, width, tri, read, weight = loop_blocks(q, k, v, g, ld, i)
+    blocks = q.shape[0] // SPAN
     strict = square(SPAN, lambda r, c: r < c).astype(F32)
     lane = lax.broadcasted_iota(jnp.int32, (heads, width), 1)
-    pick = ((lane >= HEAD_DIM * lax.broadcasted_iota(jnp.int32, (heads, width), 0))
-            & (lane < HEAD_DIM * (1 + lax.broadcasted_iota(jnp.int32, (heads, width), 0)))).astype(F32)
-
-    def sums(c):
-        part = ld[0, :, c * SPAN : (c + 1) * SPAN]
-        return dot(tri, part, 1, 1, HI), dot(part, tri, 1, 1, HI)
-
-    def shrink(row, state):
-        return jnp.concatenate(
-            [jnp.exp(row[j : j + 1, SPAN - 1 : SPAN]) * state[j * HEAD_DIM : (j + 1) * HEAD_DIM]
-             for j in range(heads)], axis=0)
-
-    cums = [sums(c) for c in range(blocks)]
-    states[0] = first_state[...]
-    for c in range(blocks - 1):
-        at = slice(c * SPAN, (c + 1) * SPAN)
-        col, row = cums[c]
-        to_end = spread(jnp.exp(col[SPAN - 1 : SPAN, :] - col), width)
-        ve = (v[at, :].astype(F32) * to_end).astype(BF16)
-        states[c + 1] = shrink(row, states[c]) + dot(ve, k[at, :], 0, 0)
-    d_state = last_grad[...]
-    for c in reversed(range(blocks)):
-        at = slice(c * SPAN, (c + 1) * SPAN)
-        col, row = cums[c]
-        qc, kc = q[at, :], k[at, :]
-        vc, gc = v[at, :], g[at, :]
-        state = states[c]
+    low = HEAD_DIM * lax.broadcasted_iota(jnp.int32, (heads, width), 0)
+    pick = ((lane >= low) & (lane < low + HEAD_DIM)).astype(F32)
+    lanes = slice(i * STATE, (i + 1) * STATE)
+
+    def one(c, state):
+        at, col, row, qc, kc, vc, gc, to_end, grown = read(c)
+        d_state = grads[i, c]
         sb, db = state.astype(BF16), d_state.astype(BF16)
-        to_end = spread(jnp.exp(col[SPAN - 1 : SPAN, :] - col), width)
-        ge32 = gc.astype(F32) * spread(jnp.exp(col), width)
+        ge32 = gc.astype(F32) * grown
         v32 = vc.astype(F32)
         ge = ge32.astype(BF16)
         ve = (v32 * to_end).astype(BF16)
-        y = dot(qc, sb, 1, 1)
-        z = dot(kc, db, 1, 1) * to_end
-        r_cross = dot(pick, ge32 * y, 1, 1, HI)
-        c_cross = dot(pick, v32 * z, 1, 1, HI)
+        r_cross = dot(pick, ge32 * dot(qc, sb, 1, 1), 1, 1, HI)
+        c_cross = dot(pick, v32 * (dot(kc, db, 1, 1) * to_end), 1, 1, HI)
         scores = dot(qc, kc, 1, 1)
         d_scores = jnp.zeros((SPAN, SPAN), F32)
-        r_in, c_in, d_values, through = [], [], [], []
+        r_in, c_in, through = [], [], []
         kept = shrink(row, state)
         for j in range(heads):
             head = slice(j * HEAD_DIM, (j + 1) * HEAD_DIM)
-            gap = jnp.minimum(col[:, j : j + 1] - row[j : j + 1, :], 0.0)
-            weight = jnp.where(causal, jnp.exp(gap), 0.0)
-            t1 = dot(gc[:, head], vc[:, head], 1, 1) * weight
+            t1 = dot(gc[:, head], vc[:, head], 1, 1) * weight(col, row, j)
             d_scores = d_scores + t1
             pairs = t1 * scores
             r_in.append(jnp.sum(pairs, axis=1, keepdims=True))
             c_in.append(jnp.sum(pairs, axis=0, keepdims=True))
-            d_values.append(dot((scores * weight).astype(BF16), gc[:, head], 0, 0))
             through.append(jnp.sum(kept[head, :] * d_state[head, :], keepdims=True))
-        dv[at, :] = (jnp.concatenate(d_values, axis=1) + z).astype(BF16)
         dsb = d_scores.astype(BF16)
-        dq[at, :] = dot(dsb, kc, 1, 0) + dot(ge, sb, 1, 0)
-        dk[at, :] = dot(dsb, qc, 0, 0) + dot(ve, db, 1, 0)
+        dq[at, lanes] = dot(dsb, kc, 1, 0) + dot(ge, sb, 1, 0)
+        dk[at, lanes] = dot(dsb, qc, 0, 0) + dot(ve, db, 1, 0)
         r_rows = dot(jnp.concatenate(r_in, axis=1), tri, 0, 0, HI)
         rest = dot(r_cross - jnp.concatenate(c_in, axis=0), tri, 1, 0, HI)
-        dd[0, :, at] = (r_rows + rest + dot(c_cross, strict, 1, 0, HI)
+        dd[i, :, at] = (r_rows + rest + dot(c_cross, strict, 1, 0, HI)
                         + jnp.concatenate(through, axis=0))
-        d_state = shrink(row, d_state) + dot(ge, qc, 0, 0)
+        return kept + dot(ve, kc, 0, 0)
+
+    lax.fori_loop(0, blocks, one, first_state[i * width : (i + 1) * width, :])
 
 
 def bits_of(n):
@@ -231,18 +255,25 @@
     return [(turn + i) % lead for i in range(lead)] + list(range(lead, bits))
 
 
-def weight_kernel(n, xt, dv, out, part, *rest):
+def weight_kernel(n, tp, xt, q, k, v, g, ld, first_state, last_grad, dq, dk, dd, out, norms,
+                  part, dv, grads, own_norm, got_norm, *rest):
     bits = bits_of(n)
-    levels, (send, recv) = rest[:bits], rest[bits:]
+    levels, (send, recv, send_n, recv_n) = rest[:bits], rest[bits:]
     streams = part.shape[0]
+    groups = ld.shape[0]
+    per_stream = ld.shape[1] * HEAD_DIM // LANES
+    refs = (q, k, v, g, ld)
     me = lax.axis_index("sp")
+    side = lax.axis_index("tp")
     mine = [lax.rem(me // (1 << b), 2) for b in range(bits)]
     partner = [me + (1 << b) * (1 - 2 * mine[b]) for b in range(bits)]
 
     barrier = pltpu.get_barrier_semaphore()
     for b in range(bits):
         pl.semaphore_signal(barrier, inc=1, device_id={"sp": partner[b]}, device_id_type=MESH)
-    pl.semaphore_wait(barrier, bits)
+    for d in range(1, tp):
+        pl.semaphore_signal(barrier, inc=1, device_id={"tp": lax.rem(side + d, tp)}, device_id_type=MESH)
+    pl.semaphore_wait(barrier, bits + tp - 1)
 
     def fill(s, spots):
         order = order_of(s, bits)
@@ -263,27 +294,72 @@
             device_id={"sp": partner[order_of(s, bits)[step]]}, device_id_type=MESH,
         )
 
-    for s in range(streams):
-        fill(s, range(n // 2, n))
-        hop(s, 0).start()
-    for s in range(streams):
-        fill(s, range(n // 2))
-    for step in range(bits):
+    def advance(team, step):
         half = n >> (step + 1)
         src = part if step == 0 else levels[step - 1]
-        for s in range(streams):
+        for s in team:
             hop(s, step).wait_recv()
             if step == bits - 1:
                 out[:, s * LANES : (s + 1) * LANES] = src[s, 0] + levels[step][s, 0]
             else:
                 levels[step][s] = levels[step][s] + src[s, 0:half]
                 hop(s, step + 1).start()
+
+    teams = [range(s, min(s + 3, streams)) for s in range(0, streams, 3)]
+    to_do = list(range(groups))
+    ready = 0
+    at_step = {}
+
+    def one_rest():
+        if to_do:
+            rest_pass(refs, to_do.pop(0), first_state, grads, dq, dk, dd)
+
+    def push():
+        for t in list(at_step):
+            advance(teams[t], at_step[t])
+            at_step[t] += 1
+            if at_step[t] == bits:
+                del at_step[t]
+
+    for t, team in enumerate(teams):
+        for s in team:
+            while ready <= s // per_stream:
+                value_pass(refs, ready, last_grad, dv, grads)
+                ready += 1
+            fill(s, range(n // 2, n))
+            hop(s, 0).start()
+        for s in team:
+            fill(s, range(n // 2))
+        push()
+        at_step[t] = 0
+    while at_step:
+        one_rest()
+        push()
+    while to_do:
+        one_rest()
+    total = jnp.sum(out[...] * out[...], axis=1, keepdims=True)
+    own_norm[...] = jnp.broadcast_to(total, own_norm.shape)
+
+    def give(d):
+        return pltpu.make_async_remote_copy(
+            own_norm, got_norm.at[d], send_n.at[d], recv_n.at[d],
+            device_id={"tp": lax.rem(side + d, tp)}, device_id_type=MESH,
+        )
+
+    for d in range(1, tp):
+        give(d).start()
     for step in range(bits):
         for s in range(streams):
             hop(s, step).wait_send()
-
-
-def on_device(n, block_input, value_weight, queries, key_rows, log_decay, out_grad):
+    for d in range(1, tp):
+        give(d).wait()
+    full = own_norm[...]
+    for d in range(1, tp):
+        full = full + got_norm[d]
+    norms[...] = full
+
+
+def on_device(n, tp, block_input, value_weight, queries, key_rows, log_decay, out_grad):
     rows, model = block_input.shape
     heads = log_decay.shape[1]
     groups = queries.shape[1] // STATE
@@ -333,39 +409,31 @@
         name="scan_states",
     )(fresh.reshape(piece), back.reshape(piece), logs)
 
-    query_grad, key_grad, rounded_grad, decay_rows = pl.pallas_call(
-        grad_kernel,
-        grid=(groups,),
-        in_specs=[by_group(STATE), by_group(STATE), by_group(width), by_group(width), ld_spec,
-                  state_spec, state_spec],
-        out_specs=[by_group(STATE), by_group(STATE), by_group(width), ld_spec],
-        out_shape=[
-            jax.ShapeDtypeStruct(queries.shape, F32), jax.ShapeDtypeStruct(queries.shape, F32),
-            jax.ShapeDtypeStruct((rows, heads * HEAD_DIM), BF16),
-            jax.ShapeDtypeStruct((groups, per_group, rows), F32),
-        ],
-        scratch_shapes=[VMEM((blocks, width, STATE), F32)],
-        compiler_params=pltpu.CompilerParams(vmem_limit_bytes=GRANT),
-        name="mixer_grads",
-    )(queries, key_rows, values, out_grad, decays,
-      before.reshape(heads * HEAD_DIM, STATE), after.reshape(heads * HEAD_DIM, STATE))
-
     own_rows, columns = model // n, heads * HEAD_DIM
     streams = columns // LANES
     bits = bits_of(n)
-    weight_grad = pl.pallas_call(
-        functools.partial(weight_kernel, n),
-        in_specs=[vm] * 2,
-        out_specs=vm,
-        out_shape=jax.ShapeDtypeStruct((own_rows, columns), F32),
-        scratch_shapes=[VMEM((streams, n, own_rows, LANES), F32)]
+    query_grad, key_grad, decay_rows, weight_grad, norms = pl.pallas_call(
+        functools.partial(weight_kernel, n, tp),
+        in_specs=[vm] * 8,
+        out_specs=[vm] * 5,
+        out_shape=[
+            jax.ShapeDtypeStruct(queries.shape, F32), jax.ShapeDtypeStruct(queries.shape, F32),
+            jax.ShapeDtypeStruct((groups, per_group, rows), F32),
+            jax.ShapeDtypeStruct((own_rows, columns), F32),
+            jax.ShapeDtypeStruct((own_rows, LANES), F32),
+        ],
+        scratch_shapes=[
+            VMEM((streams, n, own_rows, LANES), F32), VMEM((rows, columns), BF16),
+            VMEM((groups, blocks, width, STATE), F32),
+            VMEM((own_rows, LANES), F32), VMEM((tp, own_rows, LANES), F32),
+        ]
         + [VMEM((streams, n >> (b + 1), own_rows, LANES), F32) for b in range(bits)]
-        + [pltpu.SemaphoreType.DMA((streams, bits))] * 2,
+        + [pltpu.SemaphoreType.DMA((streams, bits))] * 2 + [pltpu.SemaphoreType.DMA((tp,))] * 2,
         compiler_params=pltpu.CompilerParams(collective_id=1, has_side_effects=True, vmem_limit_bytes=GRANT),
         name="weight_grad",
-    )(xt, rounded_grad)
-    row_norms = lax.psum(jnp.sum(weight_grad * weight_grad, axis=1), "tp")
-    return query_grad, key_grad, decay_rows.reshape(heads, rows).T, weight_grad, row_norms
+    )(xt, queries, key_rows, values, out_grad, decays,
+      before.reshape(heads * HEAD_DIM, STATE), after.reshape(heads * HEAD_DIM, STATE))
+    return query_grad, key_grad, decay_rows.reshape(heads, rows).T, weight_grad, norms[:, 0]
 
 
 def solution(mesh):
@@ -379,6 +447,6 @@
     )
     out_specs = (P("sp", "tp"), P("sp", "tp"), P("sp", "tp"), P("sp", "tp"), P("sp"))
     return jax.shard_map(
-        functools.partial(on_device, mesh.shape["sp"]),
+        functools.partial(on_device, mesh.shape["sp"], mesh.shape["tp"]),
         mesh=mesh, in_specs=in_specs, out_specs=out_specs, check_vma=False,
     )

time: 195 us -> 176 us (0.903)
  Pallas kernels: 183 us -> 163 us
  local copies, waits for them, and re-layouts: 7.17 us -> 12.3 us
  blocking collectives: 2.97 us -> 0 us
    pallas_call x2 -> x1, Pallas kernels: 119 us -> 99.8 us  [on_device(): pl.pallas_call(functools.partial(weight_kernel, n, tp), in_specs=[vm] * 8...]
    psum x1 -> x0, blocking collectives: 2.97 us -> none  [on_device(): row_norms = lax.psum(jnp.sum(weight_grad * weight_grad, axis=1), 'tp')]
    unnamed x3 -> x7, local copies, waits for them, and re-layouts: 1.89 us -> 4.09 us
where the time goes in v2:
time: 176 us
  Pallas kernels  163 us (93%)
  local copies, waits for them, and re-layouts  12.3 us (7%)
    pallas_call x1, Pallas kernels, on_device(): pl.pallas_call(functools.partial(weight_kernel, n, tp), in_specs=[vm] * 8...  99.8 us
    pallas_call x1, Pallas kernels, on_device(): pl.pallas_call(functools.partial(scan_kernel, n, chunk), in_specs=[vm] *...  53.4 us
    pallas_call x1, Pallas kernels, on_device(): pl.pallas_call(own_kernel, grid=(groups,), in_specs=[pl.BlockSpec((rows,...  9.86 us
    unnamed x7, local copies, waits for them, and re-layouts  4.09 us
    transpose x1, local copies, waits for them, and re-layouts, on_device(): xt = block_input.T.reshape(n, model // n, rows)  3.92 us

profile of v2, /device:TPU:0, one launch (start us, length us, event | category | flops | bytes accessed | tf_op | source)
XLA Modules:
  0.0 176.1 jit_solution(12765301181612421719)
XLA Ops:
  0.6 1.4 reshape.32.ld
  2.0 3.9 %copy.12 = bf16[2048,512]{1,0:T(8,128)(2,1)} copy(bf16[2048,512]{0,1:T(8,128)(2,1)} %bitcast.9) | data formatting | bytes 4194304 | tf_op jit(solution)/shard_map/transpose | solution.py:371
  5.9 9.9 %own_states.1 = (bf16[512,1024]{1,0:T(8,128)(2,1)}, f32[1024,128]{1,0:T(8,128)}, f32[1024,128]{1,0:T(8,128)}, f32[16,8,128]{2,1,0:T(8,128)}) custom-call(bf16[512,2048]{1,0:T(8,128)(2,1)} %x.1, bf16[2048,1024]{1,0:T(8,128)(2,1)} %w.1, bf16[512,512]{1,0:T(8,128)(2,1)} %q.3, bf16[512,512]{1,0:T(8,128)(2,1)} %k.3, f32[4,4,512]{2,1,0:T(4,128)} %reshape.32.ld, ...), custom_call_target="tpu_custom_call" | custom-call | tf_op jit(solution)/shard_map/own_states/pallas_call | solution.py:379
  15.8 53.4 %scan_states.1 = (f32[16,64,128]{2,1,0:T(8,128)}, f32[16,64,128]{2,1,0:T(8,128)}) custom-call(f32[16,64,128]{2,1,0:T(8,128)} %bitcast.12, f32[16,64,128]{2,1,0:T(8,128)} %bitcast.13, f32[16,8,128]{2,1,0:T(8,128)} %get-tuple-element.19.logs), custom_call_target="tpu_custom_call" | custom-call | tf_op jit(solution)/shard_map/scan_states/pallas_call | solution.py:401
  69.2 99.8 %weight_grad.1 = (f32[512,512]{1,0:T(8,128)}, f32[512,512]{1,0:T(8,128)}, f32[4,4,512]{2,1,0:T(4,128)}, f32[128,1024]{1,0:T(8,128)}, f32[128,128]{1,0:T(8,128)}) custom-call(bf16[16,128,512]{2,1,0:T(8,128)(2,1)} %bitcast.8, bf16[512,512]{1,0:T(8,128)(2,1)} %q.3, bf16[512,512]{1,0:T(8,128)(2,1)} %k.3, bf16[512,1024]{1,0:T(8,128)(2,1)} %get-tuple-element.16.v, ...), custom_call_target="tpu_custom_call" | custom-call | tf_op jit(solution)/shard_map/weight_grad/pallas_call | solution.py:415
  169.1 0.0 copy-start
  169.1 1.6 slice_reduce_fusion
  170.6 1.4 reshape.37
  172.0 0.0 copy-start.1
  172.0 2.3 %copy.16 = f32[512,512]{1,0:T(8,128)} copy(f32[512,512]{1,0:T(8,128)} %get-tuple-element.32) | data formatting | bytes 2097152
  174.3 0.0 copy-done
  174.3 1.0 copy.17
  175.3 0.0 copy-done.1
  175.3 0.8 copy.18
Async XLA Ops:
  169.1 5.3 %copy-start = (f32[512,512]{1,0:T(8,128)S(1)}, f32[512,512]{1,0:T(8,128)}, u32[]{:S(2)}) copy-start(f32[512,512]{1,0:T(8,128)} %get-tuple-element.33) | copy-start | bytes 3145732
  172.0 3.3 %copy-start.1 = (f32[128,1024]{1,0:T(8,128)S(1)}, f32[128,1024]{1,0:T(8,128)}, u32[]{:S(2)}) copy-start(f32[128,1024]{1,0:T(8,128)} %get-tuple-element.35) | copy-start | bytes 1572868

commit v3 on v2

--- a/solution.py
+++ b/solution.py
@@ -69,84 +69,91 @@
         logs[j] = jnp.broadcast_to(total[:, j : j + 1], logs.shape[1:])
 
 
-def scan_kernel(n, chunk, fresh, back, logs, before, after,
-                got_f, got_b, got_l, send_f, send_b, sems_out, sems_in, sems_out2, sems_in2):
+def scan_kernel(inner, outer, fresh, back, logs, before, after, got_f, got_b, got_l, send_f, send_b,
+                total, total_l, far, far_l, *sems):
     me = lax.axis_index("sp")
-    per_head = HEAD_DIM // chunk
+    near, far_at = lax.rem(me, inner), me // inner
+    per_log = inner * got_l.shape[1] // logs.shape[0]
+
+    def near_peer(d):
+        return far_at * inner + lax.rem(near + d, inner)
+
+    def far_peer(d):
+        return lax.rem(far_at + d, outer) * inner + near
 
     barrier = pltpu.get_barrier_semaphore()
-
-    def greet(d, _):
-        pl.semaphore_signal(barrier, inc=1, device_id={"sp": lax.rem(me + d, n)}, device_id_type=MESH)
-        return 0
-
-    lax.fori_loop(1, n, greet, 0)
-    pl.semaphore_wait(barrier, n - 1)
-
-    def first(d):
-        to = lax.rem(me + d, n)
+    peers = [near_peer(d) for d in range(1, inner)] + [far_peer(d) for d in range(1, outer)]
+    for to in peers:
+        pl.semaphore_signal(barrier, inc=1, device_id={"sp": to}, device_id_type=MESH)
+    pl.semaphore_wait(barrier, len(peers))
+
+    def copies(pairs, out_sem, in_sem, d, to):
         return [
             pltpu.make_async_remote_copy(
-                src, dst, sems_out.at[kind, d], sems_in.at[kind, d],
+                src, dst, out_sem.at[kind, d], in_sem.at[kind, d],
                 device_id={"sp": to}, device_id_type=MESH,
             )
-            for kind, (src, dst) in enumerate((
-                (fresh.at[to], got_f.at[me]),
-                (back.at[to], got_b.at[me]),
-                (logs.at[to // per_head], got_l.at[me]),
-            ))
+            for kind, (src, dst) in enumerate(pairs)
         ]
 
-    def go(make):
-        def body(d, _):
-            for copy in make(d):
-                copy.start()
-            return 0
-        lax.fori_loop(1, n, body, 0)
-
-    def done(make):
-        def body(d, _):
-            for copy in make(d):
-                copy.wait()
-            return 0
-        lax.fori_loop(1, n, body, 0)
-
-    go(first)
-    got_f[me] = fresh[me]
-    got_b[me] = back[me]
-    got_l[me] = logs[me // per_head]
-    done(first)
-
-    def forward(j, run):
-        send_f[j] = run
-        return jnp.exp(got_l[j][0:1, :]) * run + got_f[j]
-
-    def backward(i, run):
-        j = n - 1 - i
-        send_b[j] = run
-        return jnp.exp(got_l[j][0:1, :]) * run + got_b[j]
-
-    zero = jnp.zeros((chunk, STATE), F32)
-    lax.fori_loop(0, n, forward, zero)
-    lax.fori_loop(0, n, backward, zero)
-
-    def second(d):
-        to = lax.rem(me + d, n)
-        return [
-            pltpu.make_async_remote_copy(
-                src, dst, sems_out2.at[kind, d], sems_in2.at[kind, d],
-                device_id={"sp": to}, device_id_type=MESH,
-            )
-            for kind, (src, dst) in enumerate((
-                (send_b.at[to], after.at[me]),
-                (send_f.at[to], before.at[me]),
-            ))
-        ]
-
-    go(second)
-    before[me] = send_f[me]
-    after[me] = send_b[me]
-    done(second)
+    def log_of(to):
+        tall = got_l.shape[1]
+        return pl.ds(to // per_log if tall == 1 else to * tall, tall)
+
+    first, second, third = [], [], []
+    for d in range(1, inner):
+        to = lax.rem(near + d, inner)
+        first += copies(((fresh.at[to], got_f.at[near]), (back.at[to], got_b.at[near]),
+                         (logs.at[log_of(to)], got_l.at[near])), sems[0], sems[1], d, near_peer(d))
+        third += copies(((send_b.at[to], after.at[near]), (send_f.at[to], before.at[near])),
+                        sems[4], sems[5], d, near_peer(d))
+    for d in range(1, outer):
+        wrapped = (far_at + d) // outer
+        second += copies(((total.at[wrapped], far.at[far_at]), (total_l, far_l.at[far_at])),
+                         sems[2], sems[3], d, far_peer(d))
+
+    for copy in first:
+        copy.start()
+    got_f[near] = fresh[near]
+    got_b[near] = back[near]
+    got_l[near] = logs[log_of(near)]
+    for copy in first:
+        copy.wait()
+
+    def carry(log, run, new):
+        return jnp.exp(log[:, 0:1, :]) * run + new
+
+    ahead, behind = got_f[0], got_b[inner - 1]
+    log = got_l[0]
+    for c in range(1, inner):
+        ahead = carry(got_l[c], ahead, got_f[c])
+        behind = carry(got_l[inner - 1 - c], behind, got_b[inner - 1 - c])
+        log = log + got_l[c]
+    total[0] = ahead
+    total[1] = behind
+    total_l[...] = log
+    for copy in second:
+        copy.start()
+    for copy in second:
+        copy.wait()
+
+    zero = jnp.zeros(ahead.shape, F32)
+    run = lax.fori_loop(0, far_at, lambda j, r: carry(far_l[j], r, far[j]), zero)
+    for c in range(inner):
+        send_f[c] = run
+        run = carry(got_l[c], run, got_f[c])
+    run = lax.fori_loop(
+        0, outer - 1 - far_at,
+        lambda i, r: carry(far_l[outer - 1 - i], r, far[outer - 1 - i]), zero)
+    for c in reversed(range(inner)):
+        send_b[c] = run
+        run = carry(got_l[c], run, got_b[c])
+    for copy in third:
+        copy.start()
+    before[near] = send_f[near]
+    after[near] = send_b[near]
+    for copy in third:
+        copy.wait()
 
 
 def loop_blocks(q, k, v, g, ld, i):
@@ -365,7 +372,6 @@
     groups = queries.shape[1] // STATE
     per_group = heads // groups
     width = per_group * HEAD_DIM
-    chunk = heads * HEAD_DIM // n
     blocks = rows // SPAN
     decays = log_decay.T.reshape(groups, per_group, rows)
     xt = block_input.T.reshape(n, model // n, rows)
@@ -397,14 +403,22 @@
     )(block_input, value_weight, queries, key_rows, decays, out_grad)
 
     vm = pl.BlockSpec(memory_space=VMEM)
-    piece = (n, chunk, STATE)
+    inner = 1 << (bits_of(n) // 2)
+    outer = n // inner
+    chunk = heads * HEAD_DIM // inner
+    tall = max(1, chunk // HEAD_DIM)
+    own = (tall, chunk // tall, STATE)
+    piece = (inner, *own)
+    log = (tall, 8, LANES)
+    dma = pltpu.SemaphoreType.DMA
     before, after = pl.pallas_call(
-        functools.partial(scan_kernel, n, chunk),
+        functools.partial(scan_kernel, inner, outer),
         in_specs=[vm] * 3,
         out_specs=[vm] * 2,
         out_shape=[jax.ShapeDtypeStruct(piece, F32)] * 2,
-        scratch_shapes=[VMEM(piece, F32)] * 2 + [VMEM((n, 8, LANES), F32)] + [VMEM(piece, F32)] * 2
-        + [pltpu.SemaphoreType.DMA((3, n))] * 2 + [pltpu.SemaphoreType.DMA((2, n))] * 2,
+        scratch_shapes=[VMEM(piece, F32)] * 2 + [VMEM((inner, *log), F32)] + [VMEM(piece, F32)] * 2
+        + [VMEM((2, *own), F32), VMEM(log, F32), VMEM((outer, *own), F32), VMEM((outer, *log), F32)]
+        + [dma((3, inner))] * 2 + [dma((2, outer))] * 2 + [dma((2, inner))] * 2,
         compiler_params=pltpu.CompilerParams(collective_id=0, has_side_effects=True, vmem_limit_bytes=GRANT),
         name="scan_states",
     )(fresh.reshape(piece), back.reshape(piece), logs)

time: 176 us -> 158 us (0.90)
  Pallas kernels: 163 us -> 144 us
    pallas_call x1, Pallas kernels: 99.8 us -> 89.5 us  [on_device(): pl.pallas_call(functools.partial(weight_kernel, n, tp), in_specs=[vm] * 8...]
    pallas_call x1, Pallas kernels: 53.4 us -> 44.6 us  [on_device(): pl.pallas_call(functools.partial(scan_kernel, inner, outer), in_specs=[vm...]
where the time goes in v3:
time: 158 us; the launch traced here: 157 us
  Pallas kernels  144 us (91%)
  local copies, waits for them, and re-layouts  12.3 us (8%)
    pallas_call x1, Pallas kernels, on_device(): pl.pallas_call(functools.partial(weight_kernel, n, tp), in_specs=[vm] * 8...  89.5 us
    pallas_call x1, Pallas kernels, on_device(): pl.pallas_call(functools.partial(scan_kernel, inner, outer), in_specs=[vm...  44.6 us
    pallas_call x1, Pallas kernels, on_device(): pl.pallas_call(own_kernel, grid=(groups,), in_specs=[pl.BlockSpec((rows,...  9.86 us
    unnamed x7, local copies, waits for them, and re-layouts  4.09 us
    transpose x1, local copies, waits for them, and re-layouts, on_device(): xt = block_input.T.reshape(n, model // n, rows)  3.92 us

profile of v3, /device:TPU:0, one launch (start us, length us, event | category | flops | bytes accessed | tf_op | source)
XLA Modules:
  0.0 157.0 jit_solution(11725063950612103056)
XLA Ops:
  0.6 1.4 reshape.32.ld
  2.0 3.9 %copy.12 = bf16[2048,512]{1,0:T(8,128)(2,1)} copy(bf16[2048,512]{0,1:T(8,128)(2,1)} %bitcast.9) | data formatting | bytes 4194304 | tf_op jit(solution)/shard_map/transpose | solution.py:377
  5.9 9.9 %own_states.1 = (bf16[512,1024]{1,0:T(8,128)(2,1)}, f32[1024,128]{1,0:T(8,128)}, f32[1024,128]{1,0:T(8,128)}, f32[16,8,128]{2,1,0:T(8,128)}) custom-call(bf16[512,2048]{1,0:T(8,128)(2,1)} %x.1, bf16[2048,1024]{1,0:T(8,128)(2,1)} %w.1, bf16[512,512]{1,0:T(8,128)(2,1)} %q.3, bf16[512,512]{1,0:T(8,128)(2,1)} %k.3, f32[4,4,512]{2,1,0:T(4,128)} %reshape.32.ld, ...), custom_call_target="tpu_custom_call" | custom-call | tf_op jit(solution)/shard_map/own_states/pallas_call | solution.py:385
  15.8 44.6 %scan_states.1 = (f32[4,4,64,128]{3,2,1,0:T(8,128)}, f32[4,4,64,128]{3,2,1,0:T(8,128)}) custom-call(f32[4,4,64,128]{3,2,1,0:T(8,128)} %bitcast.12, f32[4,4,64,128]{3,2,1,0:T(8,128)} %bitcast.13, f32[16,8,128]{2,1,0:T(8,128)} %get-tuple-element.19.logs), custom_call_target="tpu_custom_call" | custom-call | tf_op jit(solution)/shard_map/scan_states/pallas_call | solution.py:414
  60.4 89.5 %weight_grad.1 = (f32[512,512]{1,0:T(8,128)}, f32[512,512]{1,0:T(8,128)}, f32[4,4,512]{2,1,0:T(4,128)}, f32[128,1024]{1,0:T(8,128)}, f32[128,128]{1,0:T(8,128)}) custom-call(bf16[16,128,512]{2,1,0:T(8,128)(2,1)} %bitcast.8, bf16[512,512]{1,0:T(8,128)(2,1)} %q.3, bf16[512,512]{1,0:T(8,128)(2,1)} %k.3, bf16[512,1024]{1,0:T(8,128)(2,1)} %get-tuple-element.16.v, ...), custom_call_target="tpu_custom_call" | custom-call | tf_op jit(solution)/shard_map/weight_grad/pallas_call | solution.py:429
  150.0 0.0 copy-start
  150.0 1.6 slice_reduce_fusion
  151.5 1.4 reshape.37
  152.9 0.0 copy-start.1
  152.9 2.3 %copy.16 = f32[512,512]{1,0:T(8,128)} copy(f32[512,512]{1,0:T(8,128)} %get-tuple-element.32) | data formatting | bytes 2097152
  155.2 0.0 copy-done
  155.2 1.0 copy.17
  156.2 0.0 copy-done.1
  156.2 0.8 copy.18
Async XLA Ops:
  150.0 5.3 %copy-start = (f32[512,512]{1,0:T(8,128)S(1)}, f32[512,512]{1,0:T(8,128)}, u32[]{:S(2)}) copy-start(f32[512,512]{1,0:T(8,128)} %get-tuple-element.33) | copy-start | bytes 3145732
  152.9 3.3 %copy-start.1 = (f32[128,1024]{1,0:T(8,128)S(1)}, f32[128,1024]{1,0:T(8,128)}, u32[]{:S(2)}) copy-start(f32[128,1024]{1,0:T(8,128)} %get-tuple-element.35) | copy-start | bytes 1572868
